TPU v7x, 32 devices: a whole 2x2x4 slice. The times are simulated.
32 devices in a mesh: sp: 8 (over z, x), tp: 4 (over y, core).
Axes of the slice: x: 2, y: 2, z: 4, core: 2. Of those that a mesh axis runs over, the one named last changes fastest.
Arguments:
- inputs: bfloat16 [4096, 4096], P('sp', 'tp'), may hold values from -6 to 6
- w_value: bfloat16 [4096, 4096], P(None, 'tp'), may hold values from -0.09375 to 0.09375
- w_gate: bfloat16 [4096, 4096], P(None, 'tp'), may hold values from -0.09375 to 0.09375
- taps: bfloat16 [31, 4096], P(None, 'tp'), may hold values from -1 to 1
- ln_gain: float32 [4096], P('tp'), may hold values from 0.1 to 1.9
- w_out: bfloat16 [4096, 4096], P(None, 'tp'), may hold values from -0.09375 to 0.09375
- grad_out: bfloat16 [4096, 4096], P('sp', 'tp'), may hold values from -6 to 6
Outputs:
- grad_input: bfloat16 [4096, 4096], P('sp', 'tp')
- grad_value_w: float32 [4096, 4096], P('sp', 'tp')
- grad_gate_w: float32 [4096, 4096], P('sp', 'tp')
- grad_out_w: float32 [4096, 4096], P('sp', 'tp')
- grad_taps: float32 [31, 4096], P(None, 'tp')
- grad_gain: float32 [4096], P('tp')
All inputs are finite; a program needn't handle non-finite values.
Results may differ from a plain program's by a relative error of at most 0.017.
Values may be sent and summed in bfloat16 or wider, within the bound.
A program may use at most 128 MiB of HBM per device.

v0:
```python
import jax
import jax.numpy as jnp
from jax import lax
from jax.sharding import PartitionSpec as P


def with_halo(cells, sides, width):
    for axis, dim in sides:
        count = lax.axis_size(axis)
        ends = count - 1
        head = lax.slice_in_dim(cells, 0, width, axis=dim)
        tail = lax.slice_in_dim(cells, cells.shape[dim] - width, cells.shape[dim], axis=dim)
        cells = jnp.concatenate(
            [
                lax.ppermute(tail, axis, [(i, (i + 1) % count) for i in range(ends)]),
                cells,
                lax.ppermute(head, axis, [((i + 1) % count, i) for i in range(ends)]),
            ],
            axis=dim,
        )
    return cells


def shifted(value, axis, steps):
    count = lax.axis_size(axis)
    leading, last = (max(0, -steps), min(count, count - steps))
    return lax.ppermute(value, axis, [(source, source + steps) for source in range(leading, last)])


def contract_tokens(left, right):
    return lax.dot_general(
        left, right, (((0,), (0,)), ((), ())), preferred_element_type=jnp.float32
    )


def contract_channels(left, right):
    return lax.dot_general(
        left, right, (((1,), (1,)), ((), ())), preferred_element_type=jnp.float32
    )


def local(inputs, w_value, w_gate, taps, ln_gain, w_out, grad_out):
    tok_rows = inputs.shape[0]
    own_width = w_value.shape[1]
    full_width = inputs.shape[1] * lax.axis_size("tp")
    radius = taps.shape[0] // 2
    full_inputs, full_grads = (
        lax.all_gather(inputs, "tp", axis=1, tiled=True),
        lax.all_gather(grad_out, "tp", axis=1, tiled=True),
    )
    pre_value = jnp.dot(full_inputs, w_value, preferred_element_type=jnp.float32)
    pre_gate = jnp.dot(full_inputs, w_gate, preferred_element_type=jnp.float32)
    gate_sigmoid = jax.nn.sigmoid(pre_gate)
    hidden = (pre_value * gate_sigmoid).astype(jnp.bfloat16)
    padded = with_halo(hidden, (("sp", 0),), radius).astype(jnp.float32)
    tap_values = taps.astype(jnp.float32)
    convolved = jnp.zeros((tok_rows, own_width), jnp.float32)
    for offset in range(taps.shape[0]):
        convolved = convolved + tap_values[offset] * padded[offset : offset + tok_rows]
    sum_first, sum_square = lax.psum(
        (jnp.sum(convolved, axis=1), jnp.sum(convolved * convolved, axis=1)), "tp"
    )
    mean = (sum_first / full_width)[:, None]
    variance = (sum_square / full_width)[:, None] - mean * mean
    inverse = lax.rsqrt(variance + 1e-06)
    normed = (convolved - mean) * inverse
    scaled = normed * ln_gain
    activated = jax.nn.silu(scaled).astype(jnp.bfloat16)
    grad_act = jnp.dot(full_grads, w_out, preferred_element_type=jnp.float32)
    sig_scaled = jax.nn.sigmoid(scaled)
    grad_scaled = grad_act * sig_scaled * (1.0 + scaled * (1.0 - sig_scaled))
    gain_part = jnp.sum(grad_scaled * normed, axis=0)
    grad_normed = grad_scaled * ln_gain
    first_sum, second_sum = lax.psum(
        (jnp.sum(grad_normed, axis=1), jnp.sum(grad_normed * normed, axis=1)), "tp"
    )
    grad_conv = inverse * (
        grad_normed
        - (first_sum / full_width)[:, None]
        - normed * (second_sum / full_width)[:, None]
    )
    tap_rows = []
    for offset in range(taps.shape[0]):
        tap_rows.append(jnp.sum(padded[offset : offset + tok_rows] * grad_conv, axis=0))
    grad_taps, grad_gain = (
        lax.psum(jnp.stack(tap_rows, axis=0).astype(jnp.bfloat16), "sp").astype(jnp.float32),
        lax.psum(gain_part.astype(jnp.bfloat16), "sp").astype(jnp.float32),
    )
    spread = jnp.zeros((tok_rows + 2 * radius, own_width), jnp.float32)
    for offset in range(taps.shape[0]):
        spread = spread + tap_values[offset] * jnp.pad(
            grad_conv, ((offset, 2 * radius - offset), (0, 0))
        )
    from_before = shifted(spread[tok_rows + radius :], "sp", 1)
    from_after = shifted(spread[:radius], "sp", -1)
    grad_hidden = spread[radius : radius + tok_rows]
    grad_hidden = grad_hidden + jnp.pad(from_before, ((0, tok_rows - radius), (0, 0)))
    grad_hidden = grad_hidden + jnp.pad(from_after, ((tok_rows - radius, 0), (0, 0)))
    grad_value = (grad_hidden * gate_sigmoid).astype(jnp.bfloat16)
    grad_gate = (grad_hidden * pre_value * gate_sigmoid * (1.0 - gate_sigmoid)).astype(jnp.bfloat16)
    partial_value = contract_channels(grad_value, w_value) + contract_channels(grad_gate, w_gate)
    grad_input = lax.psum_scatter(
        partial_value.astype(jnp.bfloat16), "tp", scatter_dimension=1, tiled=True
    )
    both_grads = jnp.concatenate([grad_value, grad_gate], axis=1)
    columns = full_inputs
    stacked = lax.psum_scatter(
        contract_tokens(columns, both_grads).astype(jnp.bfloat16),
        "sp",
        scatter_dimension=0,
        tiled=True,
    ).astype(jnp.float32)
    grad_value_w = stacked[:, :own_width]
    grad_gate_w = stacked[:, own_width:]
    columns = full_grads
    grad_out_w = lax.psum_scatter(
        contract_tokens(columns, activated).astype(jnp.bfloat16),
        "sp",
        scatter_dimension=0,
        tiled=True,
    ).astype(jnp.float32)
    return (grad_input, grad_value_w, grad_gate_w, grad_out_w, grad_taps, grad_gain)


def solution(mesh):
    in_specs = (
        P("sp", "tp"),
        P(None, "tp"),
        P(None, "tp"),
        P(None, "tp"),
        P("tp"),
        P(None, "tp"),
        P("sp", "tp"),
    )
    out_specs = (P("sp", "tp"), P("sp", "tp"), P("sp", "tp"), P("sp", "tp"), P(None, "tp"), P("tp"))
    return jax.shard_map(local, mesh=mesh, in_specs=in_specs, out_specs=out_specs, check_vma=False)
```

profile of v0, /device:TPU:0, one launch (start us, length us, event | category | flops | bytes accessed | tf_op | source)
XLA Modules:
  0.0 683.1 jit_solution(5888031741427793645)
XLA Ops:
  8.8 38.0 %all-gather.3.cloned.1.call-done = bf16[512,4096]{1,0:T(8,128)(2,1)} async-done(((bf16[512,1024]{1,0:T(8,128)(2,1)}), bf16[512,4096]{1,0:T(8,128)(2,1)}) %all-gather.3.cloned.1.call-update) | async-done | bytes 4194320 | tf_op jit(solution)/shard_map/all_gather | solution.py:48
  46.8 9.5 %add_divide_fusion.1 = f32[512,1024]{1,0:T(8,128)S(1)} fusion(bf16[512,4096]{1,0:T(8,128)(2,1)} %all-gather.3.cloned.1.call-done, bf16[4096,1024]{1,0:T(8,128)(2,1)} %param.9), kind=kOutput, calls=%fused_computation.52 | convolution fusion | flops 4296540160 | bytes 14680064 | tf_op jit(solution)/shard_map/dot_general | solution.py:52
  56.3 10.2 %multiply_convert_fusion.3 = (bf16[512,1024]{1,0:T(8,128)(2,1)S(1)}, f32[512,1024]{1,0:T(8,128)}) fusion(f32[512,1024]{1,0:T(8,128)S(1)} %add_divide_fusion.1, bf16[512,4096]{1,0:T(8,128)(2,1)S(1)} %copy-done.7, bf16[4096,1024]{1,0:T(8,128)(2,1)} %param.8), kind=kOutput, calls=%fused_computation.51 | convolution fusion | flops 4296015872 | bytes 17825792 | tf_op jit(solution)/shard_map/dot_general | solution.py:51
  66.6 3.6 collective-permute-start
  70.1 1.3 collective-permute-start.1
  71.7 4.2 collective-permute-done.1
  76.3 10.6 %multiply_reduce_fusion.33 = (f32[512]{0:T(512)S(1)}, f32[512]{0:T(512)S(1)}, f32[512,1024]{1,0:T(8,128)}) fusion(f32[542,1024]{1,0:T(8,128)S(1)} %maximum_convert_fusion, f32[1024]{0:T(1024)S(1)} %bitcast.107, f32[1024]{0:T(1024)S(1)} %bitcast.105, f32[1024]{0:T(1024)S(1)} %bitcast.103, f32[1024]{0:T(1024)S(1)} %bitcast.101, f32[1024]{0:T(1024)S(1)} %bitcast.99, ...), kind=kLoop, calls=%fused_computation.49 | loop fusion | flops 33553408 | bytes 67239936 | tf_op jit(solution)/shard_map/reduce_sum | solution.py:61
  86.9 5.8 all-reduce.34
  92.7 12.4 %multiply_reduce_fusion = (bf16[1024]{0:T(1024)(128)(2,1)}, f32[512]{0:T(512)S(1)}, f32[512]{0:T(512)S(1)}, f32[512,1024]{1,0:T(8,128)}) fusion(f32[512,1024]{1,0:T(8,128)} %get-tuple-element.55, f32[512]{0:T(512)S(1)} %get-tuple-element.96, f32[512]{0:T(512)S(1)} %get-tuple-element.95, f32[1024]{0:T(1024)S(1)} %copy-done.6, ...), kind=kOutput, calls=%fused_computation.9 | convolution fusion | flops 4303878144 | bytes 16791552 | tf_op jit(solution)/shard_map/dot_general | solution.py:69
  105.2 6.2 all-reduce.33
  111.4 6.0 multiply_reduce_fusion.18
  117.4 4.7 multiply_reduce_fusion.1
  122.5 2.7 stack.159
  125.5 10.8 %convert_bitcast_fusion.1 = bf16[4096,1024]{0,1:T(8,128)(2,1)} fusion(bf16[512,4096]{1,0:T(8,128)(2,1)} %all-gather.5.cloned.1.call-done, f32[512,1024]{1,0:T(8,128)} %get-tuple-element.55, f32[1024]{0:T(1024)S(1)} %copy-done.6, f32[512]{0:T(512)S(1)} %get-tuple-element.96, f32[512]{0:T(512)S(1)} %get-tuple-element.95), kind=kOutput, calls=%fused_computation.1 | convolution fusion | flops 4303355904 | bytes 14688256 | tf_op jit(solution)/shard_map/dot_general | solution.py:31
  136.4 1.5 copy-done.1
  137.9 10.1 %multiply_add_fusion = f32[542,1024]{1,0:T(8,128)S(1)} fusion(f32[512,1024]{1,0:T(8,128)S(1)} %copy-done.1, f32[1024]{0:T(1024)S(1)} %bitcast.108, f32[1024]{0:T(1024)S(1)} %bitcast.106, f32[1024]{0:T(1024)S(1)} %bitcast.104, f32[1024]{0:T(1024)S(1)} %bitcast.102, f32[1024]{0:T(1024)S(1)} %bitcast.100, f32[1024]{0:T(1024)S(1)} %bitcast.98, ...), kind=kLoop, calls=%fused_computation.3 | loop fusion | flops 33855488 | bytes 4444160 | tf_op jit(solution)/shard_map/add | solution.py:91
  148.1 4.3 collective-permute-start.2
  152.4 1.6 collective-permute-start.3
  154.2 4.3 collective-permute-done.3
  159.5 1.3 copy-done.8
  160.7 12.7 %convert_bitcast_fusion = bf16[4096,2048]{0,1:T(8,128)(2,1)} fusion(bf16[512,4096]{1,0:T(8,128)(2,1)S(1)} %copy-done.8, bf16[512,1024]{1,0:T(8,128)(2,1)S(1)} %get-tuple-element.57, bf16[512,1024]{1,0:T(8,128)(2,1)S(1)} %get-tuple-element.56), kind=kOutput, calls=%fused_computation | convolution fusion | flops 8602517504 | bytes 23068672 | tf_op jit(solution)/shard_map/dot_general | solution.py:31
  173.5 10.1 %fusion.15 = f32[512,4096]{1,0:T(8,128)} fusion(bf16[512,1024]{1,0:T(8,128)(2,1)S(1)} %get-tuple-element.57, bf16[4096,1024]{1,0:T(8,128)(2,1)} %param.9), kind=kOutput, calls=%fused_computation.70 | convolution fusion | flops 4294967296 | bytes 17825792 | tf_op jit(solution)/shard_map/dot_general | solution.py:37
  183.6 10.8 %add_convert_fusion = bf16[512,4096]{1,0:T(8,128)(2,1)} fusion(f32[512,4096]{1,0:T(8,128)} %fusion.15, bf16[512,1024]{1,0:T(8,128)(2,1)S(1)} %get-tuple-element.56, bf16[4096,1024]{1,0:T(8,128)(2,1)} %param.8), kind=kOutput, calls=%fused_computation.2 | convolution fusion | flops 4299161600 | bytes 22020096 | tf_op jit(solution)/shard_map/dot_general | solution.py:37
  195.6 1.3 convert_element_type.130
  196.8 1.5 convert_element_type.128
  198.3 148.5 %reduce-scatter.8.cloned.1.call-done = bf16[512,1024]{0,1:T(8,128)(2,1)} async-done(((bf16[4096,1024]{0,1:T(8,128)(2,1)}), bf16[512,1024]{0,1:T(8,128)(2,1)}) %reduce-scatter.8.cloned.1.call-update) | async-done | bytes 1048592 | tf_op jit(solution)/shard_map/reduce_scatter | solution.py:116
  346.8 2.6 copy.15
  349.4 280.4 %reduce-scatter.6.cloned.1.call-done = bf16[512,2048]{0,1:T(8,128)(2,1)} async-done(((bf16[4096,2048]{0,1:T(8,128)(2,1)}), bf16[512,2048]{0,1:T(8,128)(2,1)}) %reduce-scatter.6.cloned.1.call-update) | async-done | bytes 2097168 | tf_op jit(solution)/shard_map/reduce_scatter | solution.py:107
  629.7 3.5 fusion.11
  633.2 2.9 copy.14
  636.1 1.8 copy.13
  637.9 38.4 %reduce-scatter.4.cloned.1.call-done = bf16[512,1024]{1,0:T(8,128)(2,1)} async-done(((bf16[512,4096]{1,0:T(8,128)(2,1)}), bf16[512,1024]{1,0:T(8,128)(2,1)}) %reduce-scatter.4.cloned.1.call-update) | async-done | bytes 1048592 | tf_op jit(solution)/shard_map/reduce_scatter | solution.py:102
  (71 shorter events, 5.1 us)
Async XLA Ops:
  7.2 1.5 copy-start.5
  7.2 39.6 %all-gather.3.cloned.1.call-start = ((), (), s32[]{:S(2)}) async-start(), calls=%async_computation.3 | async-start | bytes 5242880 | tf_op jit(solution)/shard_map/all_gather | solution.py:48
  7.9 84.8 %all-gather.5.cloned.1.call-start = ((), (), s32[]{:S(2)}) async-start(), calls=%async_computation.4 | async-start | bytes 5242880 | tf_op jit(solution)/shard_map/all_gather | solution.py:49
  8.7 186.9 %all-reduce.38.cloned.1.call-start = ((), (), s32[]{:S(2)}) async-start(), calls=%async_computation.8 | async-start | bytes 135168 | tf_op jit(solution)/shard_map/psum | solution.py:86
  46.8 9.5 %copy-start.7 = (bf16[512,4096]{1,0:T(8,128)(2,1)S(1)}, bf16[512,4096]{1,0:T(8,128)(2,1)}, u32[]{:S(2)}) copy-start(bf16[512,4096]{1,0:T(8,128)(2,1)} %all-gather.3.cloned.1.call-done) | copy-start | bytes 12582916
  56.3 10.3 %copy-start.2 = (f32[512,1024]{1,0:T(8,128)}, f32[512,1024]{1,0:T(8,128)S(1)}, u32[]{:S(2)}) copy-start(f32[512,1024]{1,0:T(8,128)S(1)} %add_divide_fusion.1) | copy-start | bytes 6291460
  66.6 5.2 collective-permute-start
  70.1 5.8 collective-permute-start.1
  76.3 16.4 %copy-start.6 = (f32[1024]{0:T(1024)S(1)}, f32[1024]{0:T(1024)}, u32[]{:S(2)}) copy-start(f32[1024]{0:T(1024)} %param.11) | copy-start | bytes 12292
  117.4 4.7 copy-start
  125.2 221.6 %reduce-scatter.8.cloned.1.call-start = ((), (), s32[]{:S(2)}) async-start(), calls=%async_computation.7 | async-start | bytes 9437184 | tf_op jit(solution)/shard_map/reduce_scatter | solution.py:116
  136.3 1.6 copy-start.1
  136.3 493.4 %reduce-scatter.6.cloned.1.call-start = ((), (), s32[]{:S(2)}) async-start(), calls=%async_computation.6 | async-start | bytes 18874368 | tf_op jit(solution)/shard_map/reduce_scatter | solution.py:107
  137.9 20.6 %copy-start.3 = (f32[512,1024]{1,0:T(8,128)S(1)}, f32[512,1024]{1,0:T(8,128)}, u32[]{:S(2)}) copy-start(f32[512,1024]{1,0:T(8,128)} %copy-done.2) | copy-start | bytes 6291460
  137.9 20.6 %copy-start.4 = (f32[512,1024]{1,0:T(8,128)S(1)}, f32[512,1024]{1,0:T(8,128)}, u32[]{:S(2)}) copy-start(f32[512,1024]{1,0:T(8,128)} %get-tuple-element.98) | copy-start | bytes 6291460
  148.1 6.2 collective-permute-start.2
  152.4 6.2 collective-permute-start.3
  158.5 2.2 copy-start.8
  173.4 502.8 %reduce-scatter.4.cloned.1.call-start = ((), (), s32[]{:S(2)}) async-start(), calls=%async_computation.5 | async-start | bytes 5242880 | tf_op jit(solution)/shard_map/reduce_scatter | solution.py:102
Sparse Core Ops, SparseCore 0:
  9.5 37.1 all-gather.2
  48.3 34.4 all-gather.4
  125.3 70.1 all-reduce.37
  199.0 147.7 reduce-scatter.7
  350.4 279.2 reduce-scatter.5
  632.7 43.5 reduce-scatter.3
where the time goes:
time: 684 us; the launch traced here: 683 us
  waiting for transfers between devices  517 us (76%)
  matrix products  76.6 us (11%)
  other arithmetic  35.4 us (5%)
  local copies, waits for them, and re-layouts  16.5 us (2%)
  between operations  14.5 us (2%)
  blocking collectives  12 us (2%)
  starting transfers between devices  11.2 us (2%)
    reduce_scatter x1, waiting for transfers between devices, local(): lax.psum_scatter(contract_tokens(columns, both_grads).astype(jnp.bfloat16...  280 us
    reduce_scatter x1, waiting for transfers between devices, local(): lax.psum_scatter(contract_tokens(columns, activated).astype(jnp.bfloat16)...  148 us
    reduce_scatter x1, waiting for transfers between devices, local(): lax.psum_scatter(partial_value.astype(jnp.bfloat16), 'tp', scatter_dimens...  38.4 us
    all_gather x1, waiting for transfers between devices, local(): lax.all_gather(inputs, 'tp', axis=1, tiled=True)  38 us
    dot_general x2, matrix products, contract_tokens(): lax.dot_general(left, right, (((0,), (0,)), ((), ())), preferred_element_...  23.5 us
    dot_general x2, matrix products, contract_channels(): lax.dot_general(left, right, (((1,), (1,)), ((), ())), preferred_element_...  20.9 us
  transfers between devices with their start and end apart: 10, of which 9 were waited for; matrix products, arithmetic and copies ran while one was open for 15% of the time, Pallas kernels for 0%

commit v1 on v0

v1 whole, which is shorter than its diff:
```python
import jax
import jax.numpy as jnp
from jax import lax
from jax.sharding import Mesh, PartitionSpec as P


SP = ("outer", "pair")


def shifted(value, steps):
    count = lax.axis_size(SP)
    leading, last = (max(0, -steps), min(count, count - steps))
    return lax.ppermute(value, SP, [(source, source + steps) for source in range(leading, last)])


def with_halo(cells, width):
    head, tail = cells[:width], cells[cells.shape[0] - width :]
    return jnp.concatenate([shifted(tail, 1), cells, shifted(head, -1)], axis=0)


def swap(value):
    return lax.ppermute(value, "pair", [(0, 1), (1, 0)])


def sum_tokens(value):
    count, step = lax.axis_size(SP), 1
    while step < count:
        value = value + lax.ppermute(value, SP, [(i, i ^ step) for i in range(count)])
        step *= 2
    return value


def parity_columns(value, block, parity):
    rows, width = value.shape
    split = value.reshape(rows, width // (2 * block), 2, block)
    return lax.dynamic_index_in_dim(split, parity, 2, keepdims=False).reshape(rows, width // 2)


def contract_tokens(left, right):
    return lax.dot_general(
        left, right, (((0,), (0,)), ((), ())), preferred_element_type=jnp.float32
    )


def contract_channels(left, right):
    return lax.dot_general(
        left, right, (((1,), (1,)), ((), ())), preferred_element_type=jnp.float32
    )


def scatter_rows(value):
    return lax.psum_scatter(
        value.astype(jnp.bfloat16), "outer", scatter_dimension=0, tiled=True
    ).astype(jnp.float32)


def scatter_channels(value):
    count, me = lax.axis_size("tp"), lax.axis_index("tp")
    width = value.shape[1] // count

    def part(owner):
        return lax.dynamic_slice_in_dim(value, lax.rem(owner, count) * width, width, axis=1)

    total = part(me).astype(jnp.float32)
    for step in range(1, count):
        sent = lax.ppermute(part(me + step), "tp", [(i, (i + step) % count) for i in range(count)])
        total = total + sent.astype(jnp.float32)
    return total.astype(jnp.bfloat16)


def local(inputs, w_value, w_gate, taps, ln_gain, w_out, grad_out):
    tok_rows = inputs.shape[0]
    own_width = w_value.shape[1]
    full_width = inputs.shape[1] * lax.axis_size("tp")
    radius = taps.shape[0] // 2
    full_inputs, full_grads = (
        lax.all_gather(inputs, "tp", axis=1, tiled=True),
        lax.all_gather(grad_out, "tp", axis=1, tiled=True),
    )
    own = lax.axis_index("pair")
    block = full_width // lax.axis_size(SP)
    crossing = jnp.concatenate([parity_columns(cells, block, 1 - own) for cells in (grad_out, inputs)], axis=0)
    crossed = lax.all_gather(swap(crossing), "tp", axis=1, tiled=True)
    pair_grads = jnp.concatenate([parity_columns(full_grads, block, own), crossed[:tok_rows]], axis=0)
    own_columns, pair_columns = parity_columns(full_inputs, block, own), crossed[tok_rows:]
    pre_value = jnp.dot(full_inputs, w_value, preferred_element_type=jnp.float32)
    pre_gate = jnp.dot(full_inputs, w_gate, preferred_element_type=jnp.float32)
    gate_sigmoid = jax.nn.sigmoid(pre_gate)
    hidden = (pre_value * gate_sigmoid).astype(jnp.bfloat16)
    padded = with_halo(hidden, radius).astype(jnp.float32)
    tap_values = taps.astype(jnp.float32)
    convolved = jnp.zeros((tok_rows, own_width), jnp.float32)
    for offset in range(taps.shape[0]):
        convolved = convolved + tap_values[offset] * padded[offset : offset + tok_rows]
    sum_first, sum_square = lax.psum(
        (jnp.sum(convolved, axis=1), jnp.sum(convolved * convolved, axis=1)), "tp"
    )
    mean = (sum_first / full_width)[:, None]
    variance = (sum_square / full_width)[:, None] - mean * mean
    inverse = lax.rsqrt(variance + 1e-06)
    normed = (convolved - mean) * inverse
    scaled = normed * ln_gain
    activated = jax.nn.silu(scaled).astype(jnp.bfloat16)
    pair_activated = jnp.concatenate([activated, swap(activated)], axis=0)
    grad_act = jnp.dot(full_grads, w_out, preferred_element_type=jnp.float32)
    sig_scaled = jax.nn.sigmoid(scaled)
    grad_scaled = grad_act * sig_scaled * (1.0 + scaled * (1.0 - sig_scaled))
    gain_part = jnp.sum(grad_scaled * normed, axis=0)
    grad_normed = grad_scaled * ln_gain
    first_sum, second_sum = lax.psum(
        (jnp.sum(grad_normed, axis=1), jnp.sum(grad_normed * normed, axis=1)), "tp"
    )
    grad_conv = inverse * (
        grad_normed
        - (first_sum / full_width)[:, None]
        - normed * (second_sum / full_width)[:, None]
    )
    tap_rows = []
    for offset in range(taps.shape[0]):
        tap_rows.append(jnp.sum(padded[offset : offset + tok_rows] * grad_conv, axis=0))
    token_sums = sum_tokens(jnp.stack(tap_rows + [gain_part], axis=0))
    grad_taps, grad_gain = token_sums[:-1], token_sums[-1]
    spread = jnp.zeros((tok_rows + 2 * radius, own_width), jnp.float32)
    for offset in range(taps.shape[0]):
        spread = spread + tap_values[offset] * jnp.pad(
            grad_conv, ((offset, 2 * radius - offset), (0, 0))
        )
    from_before = shifted(spread[tok_rows + radius :], 1)
    from_after = shifted(spread[:radius], -1)
    grad_hidden = spread[radius : radius + tok_rows]
    grad_hidden = grad_hidden + jnp.pad(from_before, ((0, tok_rows - radius), (0, 0)))
    grad_hidden = grad_hidden + jnp.pad(from_after, ((tok_rows - radius, 0), (0, 0)))
    grad_value = (grad_hidden * gate_sigmoid).astype(jnp.bfloat16)
    grad_gate = (grad_hidden * pre_value * gate_sigmoid * (1.0 - gate_sigmoid)).astype(jnp.bfloat16)
    partial_value = contract_channels(grad_value, w_value) + contract_channels(grad_gate, w_gate)
    grad_input = scatter_channels(partial_value.astype(jnp.bfloat16))
    value_sum = contract_tokens(own_columns, grad_value) + contract_tokens(
        pair_columns, swap(grad_value)
    )
    gate_sum = contract_tokens(own_columns, grad_gate) + contract_tokens(
        pair_columns, swap(grad_gate)
    )
    grad_out_w = scatter_rows(contract_tokens(pair_grads, pair_activated))
    grad_value_w = scatter_rows(value_sum)
    grad_gate_w = scatter_rows(gate_sum)
    return (grad_input, grad_value_w, grad_gate_w, grad_out_w, grad_taps, grad_gain)


def solution(mesh):
    count, across = mesh.devices.shape
    fine = Mesh(mesh.devices.reshape(count // 2, 2, across), ("outer", "pair", "tp"))
    in_specs = (
        P(SP, "tp"),
        P(None, "tp"),
        P(None, "tp"),
        P(None, "tp"),
        P("tp"),
        P(None, "tp"),
        P(SP, "tp"),
    )
    out_specs = (P(SP, "tp"), P(SP, "tp"), P(SP, "tp"), P(SP, "tp"), P(None, "tp"), P("tp"))
    return jax.shard_map(local, mesh=fine, in_specs=in_specs, out_specs=out_specs, check_vma=False)
```

time: 684 us -> 405 us (0.59)
  waiting for transfers between devices: 517 us -> 192 us
  starting transfers between devices: 11.2 us -> 32.2 us
  blocking collectives: 12 us -> 23.6 us
  other arithmetic: 35.4 us -> 46.7 us
    reduce_scatter x3, waiting for transfers between devices: 467 us -> 68.9 us  [scatter_rows(): lax.psum_scatter(value.astype(jnp.bfloat16), 'outer', scatter_dimension=0...]
    ppermute x4 -> x14, waiting for transfers between devices: 9.06 us -> 116 us  [the longest x4 76.5 us: swap(): return lax.ppermute(value, 'pair', [(0, 1), (1, 0)])]
    all_gather x1, waiting for transfers between devices: 38 us -> 7.47 us  [local(): lax.all_gather(inputs, 'tp', axis=1, tiled=True)]
    ppermute x4 -> x14, starting transfers between devices: 10.7 us -> 31.8 us  [the longest x4 13.9 us: swap(): return lax.ppermute(value, 'pair', [(0, 1), (1, 0)])]
    psum x1, blocking collectives: 5.81 us -> 17.9 us  [local(): lax.psum((jnp.sum(convolved, axis=1), jnp.sum(convolved * convolved, axis...]
    convert_element_type x3 -> x5, other arithmetic: 3.08 us -> 12.9 us  [the longest x3 8.59 us: scatter_rows(): return lax.psum_scatter(value.astype(jnp.bfloat16), 'outer', scatter_dime...]
    dot_general x2 -> x5, matrix products: 23.5 us -> 23.5 us  [contract_tokens(): lax.dot_general(left, right, (((0,), (0,)), ((), ())), preferred_element_...]
  transfers between devices with their start and end apart: 10 -> 20, of which waited for: 9 -> 14; matrix products, arithmetic and copies ran while one was open for 15% -> 31% of each run, Pallas kernels for 0% -> 0%
where the time goes in v1:
time: 405 us; the launch traced here: 403 us
  waiting for transfers between devices  192 us (47%)
  matrix products  76.6 us (19%)
  other arithmetic  46.7 us (12%)
  starting transfers between devices  32.2 us (8%)
  blocking collectives  23.6 us (6%)
  local copies, waits for them, and re-layouts  17.1 us (4%)
  between operations  14.9 us (4%)
    ppermute x4, waiting for transfers between devices, swap(): return lax.ppermute(value, 'pair', [(0, 1), (1, 0)])  76.5 us
    reduce_scatter x3, waiting for transfers between devices, scatter_rows(): lax.psum_scatter(value.astype(jnp.bfloat16), 'outer', scatter_dimension=0...  68.9 us
    ppermute x3, waiting for transfers between devices, sum_tokens(): lax.ppermute(value, SP, [(i, i ^ step) for i in range(count)])  29.4 us
    dot_general x5, matrix products, contract_tokens(): lax.dot_general(left, right, (((0,), (0,)), ((), ())), preferred_element_...  23.5 us
    dot_general x2, matrix products, contract_channels(): lax.dot_general(left, right, (((1,), (1,)), ((), ())), preferred_element_...  20.9 us
    psum x1, blocking collectives, local(): lax.psum((jnp.sum(convolved, axis=1), jnp.sum(convolved * convolved, axis...  17.9 us
    ppermute x4, starting transfers between devices, swap(): return lax.ppermute(value, 'pair', [(0, 1), (1, 0)])  13.9 us
    dot_general x1, matrix products, local(): grad_act = jnp.dot(full_grads, w_out, preferred_element_type=jnp.float32)  12.4 us
  transfers between devices with their start and end apart: 20, of which 14 were waited for; matrix products, arithmetic and copies ran while one was open for 31% of the time, Pallas kernels for 0%

profile of v1, /device:TPU:0, one launch (start us, length us, event | category | flops | bytes accessed | tf_op | source)
XLA Modules:
  0.0 403.4 jit_solution(15717223119894662530)
XLA Ops:
  15.7 23.1 %collective-permute-done.7 = bf16[1024,512]{1,0:T(8,128)(2,1)S(1)} collective-permute-done((bf16[1024,512]{1,0:T(8,128)(2,1)S(1)}, bf16[1024,512]{1,0:T(8,128)(2,1)S(1)}, u32[]{:S(2)}, u32[]{:S(2)}) %collective-permute-start.7) | collective-permute-done | bytes 1048608 | tf_op jit(solution)/shard_map/ppermute | solution.py:22
  39.9 7.5 %all-gather.4.cloned.1.call-done = bf16[512,4096]{0,1:T(8,128)(2,1)} async-done(((bf16[512,1024]{0,1:T(8,128)(2,1)}), bf16[512,4096]{0,1:T(8,128)(2,1)}) %all-gather.4.cloned.1.call-update) | async-done | bytes 4194320 | tf_op jit(solution)/shard_map/all_gather | solution.py:77
  47.3 9.5 %add_divide_fusion.1 = f32[512,1024]{1,0:T(8,128)S(1)} fusion(bf16[512,4096]{0,1:T(8,128)(2,1)} %all-gather.4.cloned.1.call-done, bf16[4096,1024]{1,0:T(8,128)(2,1)} %param.9), kind=kOutput, calls=%fused_computation.58 | convolution fusion | flops 4296540160 | bytes 14680064 | tf_op jit(solution)/shard_map/dot_general | solution.py:87
  56.9 10.3 %multiply_convert_fusion.3 = (bf16[512,1024]{1,0:T(8,128)(2,1)S(1)}, f32[512,1024]{1,0:T(8,128)}) fusion(f32[512,1024]{1,0:T(8,128)S(1)} %add_divide_fusion.1, bf16[512,4096]{0,1:T(8,128)(2,1)S(1)} %copy-done.2, bf16[4096,1024]{1,0:T(8,128)(2,1)} %param.8), kind=kOutput, calls=%fused_computation.57 | convolution fusion | flops 4296015872 | bytes 17825792 | tf_op jit(solution)/shard_map/dot_general | solution.py:86
  67.2 3.6 collective-permute-start
  72.3 4.2 %collective-permute-done.1 = bf16[15,1024]{1,0:T(8,128)(2,1)S(1)} collective-permute-done((bf16[15,1024]{1,0:T(8,128)(2,1)S(1)}, bf16[15,1024]{1,0:T(8,128)(2,1)S(1)}, u32[]{:S(2)}, u32[]{:S(2)}) %collective-permute-start.1) | collective-permute-done | bytes 30752 | tf_op jit(solution)/shard_map/ppermute | solution.py:13
  76.9 10.6 %multiply_reduce_fusion.33 = (f32[512]{0:T(512)S(1)}, f32[512]{0:T(512)S(1)}, f32[512,1024]{1,0:T(8,128)}) fusion(f32[542,1024]{1,0:T(8,128)S(1)} %maximum_convert_fusion, f32[1024]{0:T(1024)S(1)} %bitcast.159, f32[1024]{0:T(1024)S(1)} %bitcast.157, f32[1024]{0:T(1024)S(1)} %bitcast.155, f32[1024]{0:T(1024)S(1)} %bitcast.153, f32[1024]{0:T(1024)S(1)} %bitcast.151, ...), kind=kLoop, calls=%fused_computation.55 | loop fusion | flops 33553408 | bytes 67239936 | tf_op jit(solution)/shard_map/reduce_sum | solution.py:96
  87.5 17.9 %all-reduce.34 = (f32[512]{0:T(512)S(1)}, f32[512]{0:T(512)S(1)}) all-reduce(f32[512]{0:T(512)S(1)} %get-tuple-element.41, f32[512]{0:T(512)S(1)} %get-tuple-element.40), channel_id=1, replica_groups=mesh['outer'=4,'pair'=2,'tp'=4] {'tp'}, use_global_device_ids=true, to_apply=%region_3.4 | all-reduce | flops 1024 | bytes 8192 | tf_op jit(solution)/shard_map/psum | solution.py:95
  105.4 12.4 %multiply_reduce_fusion = (f32[1024]{0:T(1024)S(1)}, f32[512]{0:T(512)S(1)}, f32[512]{0:T(512)S(1)}, bf16[512,1024]{1,0:T(8,128)(2,1)}, f32[512,1024]{1,0:T(8,128)}) fusion(f32[512,1024]{1,0:T(8,128)} %get-tuple-element.47, f32[512]{0:T(512)S(1)} %get-tuple-element.90, f32[512]{0:T(512)S(1)} %get-tuple-element.89, f32[1024]{0:T(1024)S(1)} %copy-done.18, ...), kind=kOutput, calls=%fused_computation.14 | convolution fusion | flops 4304926720 | bytes 17842176 | tf_op jit(solution)/shard_map/dot_general | solution.py:105
  123.3 4.0 copy.20
  127.3 15.8 %collective-permute-done.10 = bf16[512,1024]{1,0:T(8,128)(2,1)} collective-permute-done((bf16[512,1024]{1,0:T(8,128)(2,1)}, bf16[512,1024]{1,0:T(8,128)(2,1)}, u32[]{:S(2)}, u32[]{:S(2)}) %collective-permute-start.10) | collective-permute-done | bytes 1048608 | tf_op jit(solution)/shard_map/ppermute | solution.py:22
  143.1 7.8 %fusion.4 = bf16[2048,1024]{1,0:T(8,128)(2,1)} fusion(bf16[512,2048]{1,0:T(8,128)(2,1)S(1)} %slice-done, bf16[512,2048]{1,0:T(8,128)(2,1)S(1)} %copy-done.11, bf16[512,1024]{1,0:T(8,128)(2,1)} %collective-permute-done.10, bf16[512,1024]{1,0:T(8,128)(2,1)} %get-tuple-element.55), kind=kOutput, calls=%fused_computation.7 | convolution fusion | flops 4309647360 | bytes 10485760 | tf_op jit(solution)/shard_map/dot_general | solution.py:40
  151.0 5.7 %all-reduce.33 = (f32[512]{0:T(512)S(1)}, f32[512]{0:T(512)S(1)}) all-reduce(f32[512]{0:T(512)S(1)} %get-tuple-element.38, f32[512]{0:T(512)S(1)} %get-tuple-element.39), channel_id=1, replica_groups=mesh['outer'=4,'pair'=2,'tp'=4] {'tp'}, use_global_device_ids=true, to_apply=%region_7.8 | all-reduce | flops 1024 | bytes 8192 | tf_op jit(solution)/shard_map/psum | solution.py:110
  156.7 6.3 %multiply_reduce_fusion.18 = (f32[1024]{0:T(1024)S(1)}, f32[1024]{0:T(1024)S(1)}, f32[1024]{0:T(1024)S(1)}, f32[1024]{0:T(1024)S(1)}, f32[1024]{0:T(1024)S(1)}, ...) fusion(f32[542,1024]{1,0:T(8,128)S(1)} %maximum_convert_fusion,, ...), kind=kLoop, calls=%fused_computation.32 | loop fusion | flops 17288192 | bytes 33619968 | tf_op jit(solution)/shard_map/reduce_sum | solution.py:120
  163.0 10.2 %multiply_add_fusion = f32[542,1024]{1,0:T(8,128)S(1)} fusion(f32[512,1024]{1,0:T(8,128)S(1)} %get-tuple-element.46, f32[1024]{0:T(1024)S(1)} %bitcast.160, f32[1024]{0:T(1024)S(1)} %bitcast.158, f32[1024]{0:T(1024)S(1)} %bitcast.156, f32[1024]{0:T(1024)S(1)} %bitcast.154, f32[1024]{0:T(1024)S(1)} %bitcast.152, f32[1024]{0:T(1024)S(1)} %bitcast.150, ...), kind=kLoop, calls=%fused_computation.8 | loop fusion | flops 33855488 | bytes 4444160 | tf_op jit(solution)/shard_map/add | solution.py:125
  173.3 3.7 collective-permute-start.2
  178.9 4.3 %collective-permute-done.3 = f32[15,1024]{1,0:T(8,128)S(1)} collective-permute-done((f32[15,1024]{1,0:T(8,128)S(1)}, f32[15,1024]{1,0:T(8,128)S(1)}, u32[]{:S(2)}, u32[]{:S(2)}) %collective-permute-start.3) | collective-permute-done | bytes 61472 | tf_op jit(solution)/shard_map/ppermute | solution.py:13
  185.1 6.6 %collective-permute-start.8 = (bf16[512,1024]{1,0:T(8,128)(2,1)S(1)}, bf16[512,1024]{1,0:T(8,128)(2,1)S(1)}, u32[]{:S(2)}, u32[]{:S(2)}) collective-permute-start(bf16[512,1024]{1,0:T(8,128)(2,1)S(1)} %get-tuple-element.48), channel_id=1, source_target_pairs={{0,4},{4,0},{1,5},{5,1},{2,6},{6,2},{3,7},{7,3},{8,12},{12,8},{9,1... | collective-permute-start | bytes 3145736 | tf_op jit(solution)/shard_map/ppermute | solution.py:22
  191.8 21.0 %collective-permute-done.8 = bf16[512,1024]{1,0:T(8,128)(2,1)S(1)} collective-permute-done((bf16[512,1024]{1,0:T(8,128)(2,1)S(1)}, bf16[512,1024]{1,0:T(8,128)(2,1)S(1)}, u32[]{:S(2)}, u32[]{:S(2)}) %collective-permute-start.8) | collective-permute-done | bytes 1048608 | tf_op jit(solution)/shard_map/ppermute | solution.py:22
  215.3 4.4 %add_convert_fusion.1 = bf16[2048,1024]{1,0:T(8,128)(2,1)} fusion(f32[2048,1024]{1,0:T(8,128)S(1)} %fusion.12, bf16[512,2048]{0,1:T(8,128)(2,1)S(1)} %bitcast.93, bf16[512,1024]{1,0:T(8,128)(2,1)S(1)} %get-tuple-element.48), kind=kOutput, calls=%fused_computation.1 | convolution fusion | flops 2151677952 | bytes 15728640 | tf_op jit(solution)/shard_map/dot_general | solution.py:40
  221.8 4.3 %fusion.20 = f32[2048,1024]{1,0:T(8,128)S(1)} fusion(bf16[512,2048]{0,1:T(8,128)(2,1)} %bitcast.94, bf16[512,1024]{1,0:T(8,128)(2,1)} %get-tuple-element.49), kind=kOutput, calls=%fused_computation.82 | convolution fusion | flops 2147483648 | bytes 11534336 | tf_op jit(solution)/shard_map/dot_general | solution.py:40
  226.1 16.6 %collective-permute-done.9 = bf16[512,1024]{1,0:T(8,128)(2,1)S(1)} collective-permute-done((bf16[512,1024]{1,0:T(8,128)(2,1)}, bf16[512,1024]{1,0:T(8,128)(2,1)S(1)}, u32[]{:S(2)}, u32[]{:S(2)}) %collective-permute-start.9) | collective-permute-done | bytes 1048608 | tf_op jit(solution)/shard_map/ppermute | solution.py:22
  242.7 4.6 %add_convert_fusion = bf16[2048,1024]{1,0:T(8,128)(2,1)} fusion(f32[2048,1024]{1,0:T(8,128)S(1)} %fusion.20, bf16[512,1024]{1,0:T(8,128)(2,1)S(1)} %collective-permute-done.9, bf16[1024,2048]{1,0:T(8,128)(2,1)S(1)} %copy-done.13), kind=kOutput, calls=%fused_computation | convolution fusion | flops 2151677952 | bytes 15728640 | tf_op jit(solution)/shard_map/dot_general | solution.py:40
  247.3 11.5 %fusion.19 = f32[512,4096]{1,0:T(8,128)} fusion(bf16[512,1024]{1,0:T(8,128)(2,1)} %get-tuple-element.49, bf16[4096,1024]{1,0:T(8,128)(2,1)} %param.9), kind=kOutput, calls=%fused_computation.81 | convolution fusion | flops 4294967296 | bytes 17825792 | tf_op jit(solution)/shard_map/dot_general | solution.py:46
  258.8 9.4 %add_convert_fusion.2 = bf16[512,4096]{1,0:T(8,128)(2,1)S(1)} fusion(f32[512,4096]{1,0:T(8,128)} %fusion.19, bf16[512,1024]{1,0:T(8,128)(2,1)S(1)} %get-tuple-element.48, bf16[4096,1024]{1,0:T(8,128)(2,1)} %param.8), kind=kOutput, calls=%fused_computation.2 | convolution fusion | flops 4299161600 | bytes 22020096 | tf_op jit(solution)/shard_map/dot_general | solution.py:46
  273.0 4.6 %multiply_reduce_fusion.1 = (f32[1024]{0:T(1024)S(1)}, f32[1024]{0:T(1024)S(1)}, f32[1024]{0:T(1024)S(1)}, f32[1024]{0:T(1024)S(1)}, f32[1024]{0:T(1024)S(1)}, /...) fusion(f32[512,1024]{1,0:T(8,128)S(1)} %copy-done.1, ...), kind=kLoop, calls=%fused_computation.15 | loop fusion | flops 18855936 | bytes 39919616 | tf_op jit(solution)/shard_map/reduce_sum | solution.py:120
  279.4 4.1 %collective-permute-done.11 = f32[32,1024]{1,0:T(8,128)S(1)} collective-permute-done((f32[32,1024]{1,0:T(8,128)S(1)}, f32[32,1024]{1,0:T(8,128)S(1)}, u32[]{:S(2)}, u32[]{:S(2)}) %collective-permute-start.11) | collective-permute-done | bytes 131104 | tf_op jit(solution)/shard_map/ppermute | solution.py:28
  283.6 4.4 %collective-permute-start.12 = (f32[32,1024]{1,0:T(8,128)S(1)}, f32[32,1024]{1,0:T(8,128)S(1)}, u32[]{:S(2)}, u32[]{:S(2)}) collective-permute-start(f32[32,1024]{1,0:T(8,128)S(1)} %add.425), channel_id=1, source_target_pairs={{0,8},{4,12},{8,0},{12,4},{16,24},{20,28},{24,16},{28,20},{1,9},{5... | collective-permute-start | bytes 393224 | tf_op jit(solution)/shard_map/ppermute | solution.py:28
  288.0 10.6 %collective-permute-done.12 = f32[32,1024]{1,0:T(8,128)S(1)} collective-permute-done((f32[32,1024]{1,0:T(8,128)S(1)}, f32[32,1024]{1,0:T(8,128)S(1)}, u32[]{:S(2)}, u32[]{:S(2)}) %collective-permute-start.12) | collective-permute-done | bytes 131104 | tf_op jit(solution)/shard_map/ppermute | solution.py:28
  298.7 14.6 %collective-permute-done.13 = f32[32,1024]{1,0:T(8,128)S(1)} collective-permute-done((f32[32,1024]{1,0:T(8,128)S(1)}, f32[32,1024]{1,0:T(8,128)S(1)}, u32[]{:S(2)}, u32[]{:S(2)}) %collective-permute-start.13) | collective-permute-done | bytes 131104 | tf_op jit(solution)/shard_map/ppermute | solution.py:28
  314.6 4.0 %add_convert_fusion.3 = bf16[512,1024]{1,0:T(8,128)(2,1)} fusion(bf16[512,1024]{1,0:T(8,128)(2,1)} %collective-permute-done.6, bf16[512,1024]{1,0:T(8,128)(2,1)} %collective-permute-done.5, bf16[512,1024]{1,0:T(8,128)(2,1)} %collective-permute-done.4, bf16[512,4096]{1,0:T(8,128)(2,1)} %copy-done.9, s32[]{:T(128)S(6)} %select_n.22), kind=kLoop, calls=%fused_computation.47 | loop fusion | flops 4194304 | bytes 5242884 | tf_op jit(solution)/shard_map/convert_element_type | solution.py:68
  324.4 68.9 %reduce-scatter.6.cloned.1.call-done = bf16[512,1024]{1,0:T(8,128)(2,1)} async-done(((bf16[2048,1024]{1,0:T(8,128)(2,1)}), bf16[512,1024]{1,0:T(8,128)(2,1)}) %reduce-scatter.6.cloned.1.call-update) | async-done | bytes 1048592 | tf_op jit(solution)/shard_map/reduce_scatter | solution.py:52
  (98 shorter events, 41.8 us)
Async XLA Ops:
  7.2 40.2 %all-gather.4.cloned.1.call-start = ((), (), s32[]{:S(2)}) async-start(), calls=%async_computation.3 | async-start | bytes 5242880 | tf_op jit(solution)/shard_map/all_gather | solution.py:77
  9.6 95.8 %all-gather.6.cloned.1.call-start = ((), (), s32[]{:S(2)}) async-start(), calls=%async_computation.4 | async-start | bytes 5242880 | tf_op jit(solution)/shard_map/all_gather | solution.py:78
  11.1 116.2 %all-gather.8.cloned.1.call-start = ((), (), s32[]{:S(2)}) async-start(), calls=%async_computation.5 | async-start | bytes 5242880 | tf_op jit(solution)/shard_map/all_gather | solution.py:83
  12.6 26.2 %collective-permute-start.7 = (bf16[1024,512]{1,0:T(8,128)(2,1)S(1)}, bf16[1024,512]{1,0:T(8,128)(2,1)S(1)}, u32[]{:S(2)}, u32[]{:S(2)}) collective-permute-start(bf16[1024,512]{1,0:T(8,128)(2,1)S(1)} %pad_maximum_fusion), channel_id=1, source_target_pairs={{0,4},{4,0},{1,5},{5,1},{2,6},{6,2},{3,7},{7,3},{8,12},{12,8},{9,1... | collective-permute-start | bytes 3145736 | tf_op jit(solution)/shard_map/ppermute | solution.py:22
  39.8 278.8 %reduce-scatter.8.cloned.1.call-start = ((), (), s32[]{:S(2)}) async-start(), calls=%async_computation.8 | async-start | bytes 5242880 | tf_op jit(solution)/shard_map/reduce_scatter | solution.py:52
  47.3 9.5 %copy-start.2 = (bf16[512,4096]{0,1:T(8,128)(2,1)S(1)}, bf16[512,4096]{0,1:T(8,128)(2,1)}, u32[]{:S(2)}) copy-start(bf16[512,4096]{0,1:T(8,128)(2,1)} %all-gather.4.cloned.1.call-done) | copy-start | bytes 12582916
  56.9 10.3 %copy-start.4 = (f32[512,1024]{1,0:T(8,128)}, f32[512,1024]{1,0:T(8,128)S(1)}, u32[]{:S(2)}) copy-start(f32[512,1024]{1,0:T(8,128)S(1)} %add_divide_fusion.1) | copy-start | bytes 6291460
  67.2 5.2 %collective-permute-start = (bf16[15,1024]{1,0:T(8,128)(2,1)S(1)}, bf16[15,1024]{1,0:T(8,128)(2,1)S(1)}, u32[]{:S(2)}, u32[]{:S(2)}) collective-permute-start(bf16[15,1024]{1,0:T(8,128)(2,1)S(1)} %get-tuple-element.56), channel_id=1, source_target_pairs={{0,4},{4,8},{8,12},{12,16},{16,20},{20,24},{24,28},{1,5},{5,9},{9,... | collective-permute-start | bytes 92168 | tf_op jit(solution)/shard_map/ppermute | solution.py:13
  70.7 5.8 %collective-permute-start.1 = (bf16[15,1024]{1,0:T(8,128)(2,1)S(1)}, bf16[15,1024]{1,0:T(8,128)(2,1)S(1)}, u32[]{:S(2)}, u32[]{:S(2)}) collective-permute-start(bf16[15,1024]{1,0:T(8,128)(2,1)S(1)} %get-tuple-element.57), channel_id=1, source_target_pairs={{4,0},{8,4},{12,8},{16,12},{20,16},{24,20},{28,24},{5,1},{9,5},{13... | collective-permute-start | bytes 92168 | tf_op jit(solution)/shard_map/ppermute | solution.py:13
  76.9 28.5 %copy-start.18 = (f32[1024]{0:T(1024)S(1)}, f32[1024]{0:T(1024)}, u32[]{:S(2)}) copy-start(f32[1024]{0:T(1024)} %param.11) | copy-start | bytes 12292
  117.8 25.3 %collective-permute-start.10 = (bf16[512,1024]{1,0:T(8,128)(2,1)}, bf16[512,1024]{1,0:T(8,128)(2,1)}, u32[]{:S(2)}, u32[]{:S(2)}) collective-permute-start(bf16[512,1024]{1,0:T(8,128)(2,1)} %get-tuple-element.55), channel_id=1, source_target_pairs={{0,4},{4,0},{1,5},{5,1},{2,6},{6,2},{3,7},{7,3},{8,12},{12,8},{9,1... | collective-permute-start | bytes 3145736 | tf_op jit(solution)/shard_map/ppermute | solution.py:22
  127.3 15.9 %copy-start.11 = (bf16[512,2048]{1,0:T(8,128)(2,1)S(1)}, bf16[512,2048]{1,0:T(8,128)(2,1)}, u32[]{:S(2)}) copy-start(bf16[512,2048]{1,0:T(8,128)(2,1)} %copy.20) | copy-start | bytes 6291460
  127.3 15.9 %slice-start = ((bf16[1024,2048]{1,0:T(8,128)(2,1)}), bf16[512,2048]{1,0:T(8,128)(2,1)S(1)}, s32[]{:S(2)}) async-start(bf16[1024,2048]{1,0:T(8,128)(2,1)} %all-gather.8.cloned.1.call-done), calls=%async_computation.9 | async-start | bytes 4194304 | tf_op jit(solution)/shard_map/slice | solution.py:84
  150.9 170.5 %reduce-scatter.4.cloned.1.call-start = ((), (), s32[]{:S(2)}) async-start(), calls=%async_computation.6 | async-start | bytes 5242880 | tf_op jit(solution)/shard_map/reduce_scatter | solution.py:52
  163.0 10.3 %copy-start = (f32[512,1024]{1,0:T(8,128)}, f32[512,1024]{1,0:T(8,128)S(1)}, u32[]{:S(2)}) copy-start(f32[512,1024]{1,0:T(8,128)S(1)} %get-tuple-element.46) | copy-start | bytes 6291460
  163.0 20.2 %copy-start.5 = (f32[512,1024]{1,0:T(8,128)S(1)}, f32[512,1024]{1,0:T(8,128)}, u32[]{:S(2)}) copy-start(f32[512,1024]{1,0:T(8,128)} %copy-done.4) | copy-start | bytes 6291460
  163.0 20.1 %copy-start.6 = (f32[512,1024]{1,0:T(8,128)S(1)}, f32[512,1024]{1,0:T(8,128)}, u32[]{:S(2)}) copy-start(f32[512,1024]{1,0:T(8,128)} %get-tuple-element.92) | copy-start | bytes 6291460
  173.3 5.6 %collective-permute-start.2 = (f32[15,1024]{1,0:T(8,128)S(1)}, f32[15,1024]{1,0:T(8,128)S(1)}, u32[]{:S(2)}, u32[]{:S(2)}) collective-permute-start(f32[15,1024]{1,0:T(8,128)S(1)} %get-tuple-element.53), channel_id=1, source_target_pairs={{0,4},{4,8},{8,12},{12,16},{16,20},{20,24},{24,28},{1,5},{5,9},{9,... | collective-permute-start | bytes 184328 | tf_op jit(solution)/shard_map/ppermute | solution.py:13
  177.0 6.2 %collective-permute-start.3 = (f32[15,1024]{1,0:T(8,128)S(1)}, f32[15,1024]{1,0:T(8,128)S(1)}, u32[]{:S(2)}, u32[]{:S(2)}) collective-permute-start(f32[15,1024]{1,0:T(8,128)S(1)} %get-tuple-element.54), channel_id=1, source_target_pairs={{4,0},{8,4},{12,8},{16,12},{20,16},{24,20},{28,24},{5,1},{9,5},{13... | collective-permute-start | bytes 184328 | tf_op jit(solution)/shard_map/ppermute | solution.py:13
  183.2 8.5 %copy-start.3 = (bf16[512,4096]{0,1:T(8,128)(2,1)S(1)}, bf16[512,4096]{0,1:T(8,128)(2,1)}, u32[]{:S(2)}) copy-start(bf16[512,4096]{0,1:T(8,128)(2,1)} %all-gather.4.cloned.1.call-done) | copy-start | bytes 12582916
  185.1 27.8 %collective-permute-start.8 = (bf16[512,1024]{1,0:T(8,128)(2,1)S(1)}, bf16[512,1024]{1,0:T(8,128)(2,1)S(1)}, u32[]{:S(2)}, u32[]{:S(2)}) collective-permute-start(bf16[512,1024]{1,0:T(8,128)(2,1)S(1)} %get-tuple-element.48), channel_id=1, source_target_pairs={{0,4},{4,0},{1,5},{5,1},{2,6},{6,2},{3,7},{7,3},{8,12},{12,8},{9,1... | collective-permute-start | bytes 3145736 | tf_op jit(solution)/shard_map/ppermute | solution.py:22
  191.7 21.2 %copy-start.12 = (bf16[1024,2048]{1,0:T(8,128)(2,1)S(1)}, bf16[1024,2048]{1,0:T(8,128)(2,1)}, u32[]{:S(2)}) copy-start(bf16[1024,2048]{1,0:T(8,128)(2,1)} %all-gather.8.cloned.1.call-done) | copy-start | bytes 12582916
  191.8 23.5 %copy-start.10 = (bf16[512,4,1,512]{0,3,2,1:T(8,128)(2,1)}, bf16[512,4,1,512]{0,3,2,1:T(8,128)(2,1)S(1)}, u32[]{:S(2)}) copy-start(bf16[512,4,1,512]{0,3,2,1:T(8,128)(2,1)S(1)} %constant_dynamic-slice_fusion.3) | copy-start | bytes 6291460
  219.7 173.6 %reduce-scatter.6.cloned.1.call-start = ((), (), s32[]{:S(2)}) async-start(), calls=%async_computation.7 | async-start | bytes 5242880 | tf_op jit(solution)/shard_map/reduce_scatter | solution.py:52
  220.0 22.7 %copy-start.13 = (bf16[1024,2048]{1,0:T(8,128)(2,1)S(1)}, bf16[1024,2048]{1,0:T(8,128)(2,1)}, u32[]{:S(2)}) copy-start(bf16[1024,2048]{1,0:T(8,128)(2,1)} %all-gather.8.cloned.1.call-done) | copy-start | bytes 12582916
  220.0 22.7 %collective-permute-start.9 = (bf16[512,1024]{1,0:T(8,128)(2,1)}, bf16[512,1024]{1,0:T(8,128)(2,1)S(1)}, u32[]{:S(2)}, u32[]{:S(2)}) collective-permute-start(bf16[512,1024]{1,0:T(8,128)(2,1)} %get-tuple-element.49), channel_id=1, source_target_pairs={{0,4},{4,0},{1,5},{5,1},{2,6},{6,2},{3,7},{7,3},{8,12},{12,8},{9,1... | collective-permute-start | bytes 3145736 | tf_op jit(solution)/shard_map/ppermute | solution.py:22
  271.0 43.0 %collective-permute-start.4 = (bf16[512,1024]{1,0:T(8,128)(2,1)}, bf16[512,1024]{1,0:T(8,128)(2,1)}, u32[]{:S(2)}, u32[]{:S(2)}) collective-permute-start(bf16[512,1024]{1,0:T(8,128)(2,1)} %get-tuple-element.50), channel_id=1, source_target_pairs={{0,1},{1,2},{2,3},{3,0},{4,5},{5,6},{6,7},{7,4},{8,9},{9,10},{10,1... | collective-permute-start | bytes 3145736 | tf_op jit(solution)/shard_map/ppermute | solution.py:66
  271.0 43.0 %collective-permute-start.6 = (bf16[512,1024]{1,0:T(8,128)(2,1)}, bf16[512,1024]{1,0:T(8,128)(2,1)}, u32[]{:S(2)}, u32[]{:S(2)}) collective-permute-start(bf16[512,1024]{1,0:T(8,128)(2,1)} %get-tuple-element.51), channel_id=1, source_target_pairs={{0,3},{1,0},{2,1},{3,2},{4,7},{5,4},{6,5},{7,6},{8,11},{9,8},{10,9... | collective-permute-start | bytes 3145736 | tf_op jit(solution)/shard_map/ppermute | solution.py:66
  273.0 41.6 %collective-permute-start.5 = (bf16[512,1024]{1,0:T(8,128)(2,1)S(1)}, bf16[512,1024]{1,0:T(8,128)(2,1)}, u32[]{:S(2)}, u32[]{:S(2)}) collective-permute-start(bf16[512,1024]{1,0:T(8,128)(2,1)S(1)} %get-tuple-element.52), channel_id=1, source_target_pairs={{0,2},{1,3},{2,0},{3,1},{4,6},{5,7},{6,4},{7,5},{8,10},{9,11},{10,... | collective-permute-start | bytes 3145736 | tf_op jit(solution)/shard_map/ppermute | solution.py:66
  277.9 5.7 %collective-permute-start.11 = (f32[32,1024]{1,0:T(8,128)S(1)}, f32[32,1024]{1,0:T(8,128)S(1)}, u32[]{:S(2)}, u32[]{:S(2)}) collective-permute-start(f32[32,1024]{1,0:T(8,128)S(1)} %stack.131), channel_id=1, source_target_pairs={{0,4},{4,0},{8,12},{12,8},{16,20},{20,16},{24,28},{28,24},{1,5},{5... | collective-permute-start | bytes 393224 | tf_op jit(solution)/shard_map/ppermute | solution.py:28
  283.6 15.0 %collective-permute-start.12 = (f32[32,1024]{1,0:T(8,128)S(1)}, f32[32,1024]{1,0:T(8,128)S(1)}, u32[]{:S(2)}, u32[]{:S(2)}) collective-permute-start(f32[32,1024]{1,0:T(8,128)S(1)} %add.425), channel_id=1, source_target_pairs={{0,8},{4,12},{8,0},{12,4},{16,24},{20,28},{24,16},{28,20},{1,9},{5... | collective-permute-start | bytes 393224 | tf_op jit(solution)/shard_map/ppermute | solution.py:28
  298.7 14.7 %collective-permute-start.13 = (f32[32,1024]{1,0:T(8,128)S(1)}, f32[32,1024]{1,0:T(8,128)S(1)}, u32[]{:S(2)}, u32[]{:S(2)}) collective-permute-start(f32[32,1024]{1,0:T(8,128)S(1)} %add.426), channel_id=1, source_target_pairs={{0,16},{4,20},{8,24},{12,28},{16,0},{20,4},{24,8},{28,12},{1,17},{... | collective-permute-start | bytes 393224 | tf_op jit(solution)/shard_map/ppermute | solution.py:28
  (8 other events, 22.4 us)
Sparse Core Ops, SparseCore 0:
  10.1 37.1 all-gather.3
  48.9 34.4 all-gather.5
  85.0 34.6 all-gather.7
  151.1 77.8 reduce-scatter.7
  231.1 82.5 reduce-scatter.3
  315.8 77.4 reduce-scatter.5
